TPU v7x, 32 devices: a whole 2x2x4 slice. The times are simulated.
32 devices in a mesh: ep: 8 (over z, y), tp: 4 (over x, core).
Axes of the slice: x: 2, y: 2, z: 4, core: 2. Of those that a mesh axis runs over, the one named last changes fastest.
Arguments:
- queries: bfloat16 [4096, 1024], P('ep', 'tp'), may hold values from -6 to 6
- keys: bfloat16 [4096, 512], P('ep', 'tp'), may hold values from -6 to 6
- values: bfloat16 [4096, 512], P('ep', 'tp'), may hold values from -6 to 6
- forget_cache: float32 [8, 4096], P('tp'), may hold values from -412 to 0, as said below
- query_gain: float32 [128], replicated, may hold values from 0.6 to 6
- key_gain: float32 [128], replicated, may hold values from 0.6 to 6
- mixer_out: bfloat16 [1024, 2048], replicated, may hold values from -0.75 to 0.75
- expert_input: bfloat16 [4096, 2048], P(('ep', 'tp')), may hold values from -6 to 6
- norm_gain: float32 [2048], replicated, may hold values from 0.1 to 1.9
- routes: int32 [4096, 2], P(('ep', 'tp')), may hold values from 0 to 31, all different within a row; in each aligned block of 128 rows (0 to 127, 128 to 255, ...) at most 16 rows name the same one
- route_weights: float32 [4096, 2], P(('ep', 'tp')), may hold values from 0.1 to 1
- w_gate: bfloat16 [32, 2048, 1024], P('ep', None, 'tp'), may hold values from -0.125 to 0.125
- w_up: bfloat16 [32, 2048, 1024], P('ep', None, 'tp'), may hold values from -0.125 to 0.125
- w_down: bfloat16 [32, 2048, 1024], P('ep', None, 'tp'), may hold values from -0.1875 to 0.1875
Outputs:
- mixed: bfloat16 [4096, 2048], P(('ep', 'tp'))
- routed: bfloat16 [4096, 2048], P(('ep', 'tp'))
Inputs may be any that keep to these rules, and one draw needn't show every extreme that they name: `routes`: each row names 2 different experts; among the rows of one device no expert is named by more than 16 rows, a bound that some block reaches. `forget_cache`: never rises along the positions.
All inputs are finite; a program needn't handle non-finite values.
Results may differ from a plain program's by a relative error of at most 0.013.
The roundings to bfloat16 on the way count: a program that leaves them out, or rounds other values in their place, can miss the bound.
Values may be sent and summed in bfloat16 or wider, within the bound.
A program may use at most 128 MiB of HBM per device.

v0:
```python
import math
import jax
import jax.numpy as jnp
from jax import lax
from jax.sharding import PartitionSpec as P

EXPERTS = 32
CAP = 16
EPSILON = 1e-06
NEGATIVE = -1e30


def rms_scale(inputs, gain):
    inputs = inputs.astype(jnp.float32)
    return inputs * lax.rsqrt(jnp.mean(inputs * inputs, axis=-1, keepdims=True) + EPSILON) * gain


def attend(queries, keys, values, forget_cache, query_gain, key_gain):
    rows = queries.shape[0]
    head_dim = keys.shape[1]
    local_heads = forget_cache.shape[0]
    first = lax.axis_index("ep") * rows
    normed_q = rms_scale(queries.reshape(rows, local_heads, head_dim), query_gain).astype(
        jnp.bfloat16
    )
    normed_k = rms_scale(keys, key_gain).astype(jnp.bfloat16)
    scale = head_dim ** (-0.5)
    groups = [(normed_q, first + jnp.arange(rows, dtype=jnp.int32))]
    gate_sets = [jnp.take(forget_cache, position, axis=1) for _, position in groups]
    initial = tuple(
        (
            (
                jnp.full((local_heads, group_rows.shape[0]), NEGATIVE, jnp.float32),
                jnp.zeros((local_heads, group_rows.shape[0]), jnp.float32),
                jnp.zeros((local_heads, group_rows.shape[0], head_dim), jnp.float32),
            )
            for group_rows, _ in groups
        )
    )
    key_matrix_rows = lax.all_gather(normed_k, "ep", axis=0, tiled=True)
    value_rows = lax.all_gather(values, "ep", axis=0, tiled=True)
    length = key_matrix_rows.shape[0]
    width = math.gcd(length, 512)
    query_rows, query_pos = groups[0]
    query_gates = gate_sets[0]
    last_pos = jnp.max(query_pos)

    def one_block(number, inner):
        begin = number * width

        def update(current):
            highest, denom, accum = current
            block_keys = lax.dynamic_slice_in_dim(key_matrix_rows, number * width, width, 0)
            block_values = lax.dynamic_slice_in_dim(value_rows, number * width, width, 0)
            key_gates = lax.dynamic_slice_in_dim(forget_cache, begin, width, 1)
            scores = (
                jnp.einsum(
                    "qhd,kd->hqk", query_rows, block_keys, preferred_element_type=jnp.float32
                )
                * scale
            )
            scores = scores + query_gates[:, :, None] - key_gates[:, None, :]
            key_pos = begin + jnp.arange(width, dtype=jnp.int32)
            allowed = key_pos[None, :] <= query_pos[:, None]
            scores = jnp.where(allowed[None], scores, NEGATIVE)
            newest = jnp.maximum(highest, jnp.max(scores, axis=2))
            weights = jnp.where(allowed[None], jnp.exp(scores - newest[:, :, None]), 0.0)
            factor = jnp.exp(highest - newest)
            denom = denom * factor + jnp.sum(weights, axis=2)
            product = jnp.einsum(
                "hqk,kd->hqd",
                weights.astype(jnp.bfloat16),
                block_values,
                preferred_element_type=jnp.float32,
            )
            accum = accum * factor[:, :, None] + product
            return (newest, denom, accum)

        return lax.cond(begin <= last_pos, update, lambda current: current, inner)

    results = [lax.fori_loop(0, length // width, one_block, initial[0])]
    finals = tuple(results)
    outputs = [(accum / denom[:, :, None]).astype(jnp.bfloat16) for _, denom, accum in finals]
    return outputs[0]


def dispatch(expert_input, norm_gain, routes):
    rows = expert_input.shape[0]
    top = routes.shape[1]
    normed = rms_scale(expert_input, norm_gain).astype(jnp.bfloat16)
    flat = routes.reshape(-1)
    onehot = (flat[:, None] == jnp.arange(EXPERTS, dtype=jnp.int32)[None, :]).astype(jnp.int32)
    prior_state = jnp.cumsum(onehot, axis=0) - onehot
    rank = jnp.sum(prior_state * onehot, axis=1)
    slots = rank * EXPERTS + flat
    owner = (
        jnp.full((CAP * EXPERTS,), rows, jnp.int32)
        .at[slots]
        .set(jnp.arange(rows * top, dtype=jnp.int32) // top)
    )
    padded = jnp.concatenate([normed, jnp.zeros((1, normed.shape[1]), jnp.bfloat16)], axis=0)
    outgoing = padded[owner].reshape(CAP, EXPERTS, normed.shape[1])
    received = lax.all_to_all(outgoing, "ep", split_axis=1, concat_axis=0, tiled=True)
    return (received, slots)


def on_device(
    queries,
    keys,
    values,
    forget_cache,
    query_gain,
    key_gain,
    mixer_out,
    expert_input,
    norm_gain,
    routes,
    route_weights,
    w_gate,
    w_up,
    w_down,
):
    attended = attend(queries, keys, values, forget_cache, query_gain, key_gain)
    received, slots = dispatch(expert_input, norm_gain, routes)
    regrouped = lax.all_to_all(attended, "tp", split_axis=1, concat_axis=0, tiled=True)
    all_heads = regrouped.shape[0]
    projection = mixer_out.reshape(all_heads, regrouped.shape[2], mixer_out.shape[1])
    mixed = jnp.einsum(
        "hqd,hde->qe", regrouped, projection, preferred_element_type=jnp.float32
    ).astype(jnp.bfloat16)
    pieces = lax.all_gather(received, "tp", axis=0, tiled=True)
    gate = jnp.einsum("red,edf->ref", pieces, w_gate, preferred_element_type=jnp.float32)
    upward = jnp.einsum("red,edf->ref", pieces, w_up, preferred_element_type=jnp.float32)
    hidden = (jax.nn.silu(gate) * upward).astype(jnp.bfloat16)
    summed = lax.psum_scatter(
        jnp.einsum("ref,edf->red", hidden, w_down, preferred_element_type=jnp.float32).astype(
            jnp.bfloat16
        ),
        "tp",
        scatter_dimension=0,
        tiled=True,
    )
    returned = lax.all_to_all(summed, "ep", split_axis=0, concat_axis=1, tiled=True)
    flat_back = returned.reshape(-1, returned.shape[2])
    picked = (
        flat_back[slots]
        .reshape(routes.shape[0], routes.shape[1], returned.shape[2])
        .astype(jnp.float32)
    )
    routed = jnp.sum(picked * route_weights[:, :, None], axis=1).astype(jnp.bfloat16)
    return (mixed, routed)


def solution(mesh):
    in_specs = (
        P("ep", "tp"),
        P("ep", "tp"),
        P("ep", "tp"),
        P("tp", None),
        P(),
        P(),
        P(),
        P(("ep", "tp"), None),
        P(),
        P(("ep", "tp"), None),
        P(("ep", "tp"), None),
        P("ep", None, "tp"),
        P("ep", None, "tp"),
        P("ep", None, "tp"),
    )
    out_specs = (P(("ep", "tp"), None), P(("ep", "tp"), None))
    return jax.shard_map(
        on_device, mesh=mesh, in_specs=in_specs, out_specs=out_specs, check_vma=False
    )
```

profile of v0, /device:TPU:0, one launch (start us, length us, event | category | flops | bytes accessed | tf_op | source)
XLA Modules:
  0.0 367.3 jit_solution(14982361686460898123)
XLA Ops:
  7.2 0.0 all-gather.8.cloned.1.call-start
  7.2 0.8 copy.60
  8.0 0.1 eq.29
  8.1 0.1 eq.25
  8.3 0.1 reshape.154
  8.4 0.6 reduce-window.6
  9.0 0.2 slice_reduce_fusion
  9.3 0.1 fusion.33
  9.4 1.4 scatter_custom_fusion
  10.8 1.2 fusion.22
  12.1 1.2 fusion.24
  13.4 2.5 gather_fusion.1
  15.8 1.2 copy.64
  17.0 55.3 %all_to_all.51 = bf16[16,32,2048]{2,0,1:T(8,128)(2,1)S(1)} all-to-all(bf16[16,32,2048]{2,0,1:T(8,128)(2,1)S(1)} %copy.64), channel_id=1, replica_groups=mesh['ep'=8,'tp'=4] {'ep'}, dimensions={1} | all-to-all | bytes 4194304 | tf_op jit(solution)/shard_map/all_to_all | solution.py:103
  72.3 1.5 copy.65
  73.8 0.0 all-gather.8.cloned.1.call-update
  73.8 0.0 all-gather.4.cloned.1.call-start
  73.9 0.8 copy-done
  74.7 0.1 fusion.28
  74.9 0.8 fusion.30
  75.7 0.0 all-gather.4.cloned.1.call-update
  75.7 0.0 all-gather.6.cloned.1.call-start
  75.8 0.7 all-gather.6.cloned.1.call-update
  76.5 0.2 reduce-scatter.2.cloned.1.call-start
  76.7 54.6 %all-gather.8.cloned.1.call-done = bf16[512,4,2048]{2,0,1:T(8,128)(2,1)} async-done(((bf16[128,4,2048]{2,0,1:T(8,128)(2,1)}), bf16[512,4,2048]{2,0,1:T(8,128)(2,1)}) %all-gather.8.cloned.1.call-update) | async-done | bytes 8388624 | tf_op jit(solution)/shard_map/all_gather | solution.py:131
  131.3 6.9 %fusion.42 = f32[4,512,256]{2,1,0:T(8,128)S(1)} fusion(bf16[512,4,2048]{2,0,1:T(8,128)(2,1)} %all-gather.8.cloned.1.call-done, bf16[4,2048,256]{2,1,0:T(8,128)(2,1)} %param.29), kind=kOutput, calls=%fused_computation.89 | convolution fusion | flops 2147483648 | bytes 14680064 | tf_op jit(solution)/shard_map/red,edf->ref/dot_general | solution.py:132
  138.2 14.0 %convert_bitcast_fusion = bf16[512,4,2048]{2,0,1:T(8,128)(2,1)} fusion(bf16[4,2048,256]{2,1,0:T(8,128)(2,1)} %param.31, f32[4,512,256]{2,1,0:T(8,128)S(1)} %fusion.42, bf16[512,4,2048]{2,0,1:T(8,128)(2,1)} %all-gather.8.cloned.1.call-done, bf16[4,2048,256]{2,1,0:T(8,128)(2,1)} %param.30), kind=kOutput, calls=%fused_computation.28 | convolution fusion | flops 4302307328 | bytes 27262976 | tf_op jit(solution)/shard_map/ref,edf->red/dot_general | solution.py:136
  152.2 0.0 reduce-scatter.2.cloned.1.call-update
  152.2 0.0 copy-start.1
  152.2 0.0 copy-start.5
  152.2 0.7 copy-done.2
  153.0 0.7 copy.55
  153.6 0.6 fusion.35
  154.2 1.0 gather_fusion
  155.3 0.1 select_bitcast_fusion
  155.4 0.1 copy.57
  155.5 0.0 copy-done.1
  155.5 0.2 copy.54
  155.7 0.1 fusion.25
  155.8 0.1 fusion.27
  155.9 0.2 copy.56
  156.1 18.2 %all-gather.4.cloned.1.call-done = bf16[4096,128]{1,0:T(8,128)(2,1)} async-done(((bf16[512,128]{1,0:T(8,128)(2,1)}), bf16[4096,128]{1,0:T(8,128)(2,1)}) %all-gather.4.cloned.1.call-update) | async-done | bytes 1048592 | tf_op jit(solution)/shard_map/all_gather | solution.py:40
  174.3 41.2 %all-gather.6.cloned.1.call-done = bf16[4096,128]{1,0:T(8,128)(2,1)} async-done(((bf16[512,128]{1,0:T(8,128)(2,1)}), bf16[4096,128]{1,0:T(8,128)(2,1)}) %all-gather.6.cloned.1.call-update) | async-done | bytes 1048592 | tf_op jit(solution)/shard_map/all_gather | solution.py:41
  215.5 8.8 %while.18 = (s32[]{:T(128)}, f32[2,512]{1,0:T(2,128)S(1)}, f32[2,512]{1,0:T(2,128)S(1)}, f32[2,512,128]{2,1,0:T(8,128)S(1)}, s32[]{:T(128)}, /*index=5*/bf16[409...) while((s32[]{:T(128)}, f32[2,512]{1,0:T(2,128)S(1)}, ...), condition=%wide.region_8.9_spmd.clone, body=%wide.region_3.8_spmd.clone.sunk | while | flops 274729984 | bytes 9007507 | solution.py:81
  216.1 4.0 %conditional.3 = ((f32[2,512]{1,0:T(2,128)S(1)}, f32[2,512]{1,0:T(2,128)S(1)}, f32[2,512,128]{2,1,0:T(8,128)S(1)})) conditional(s32[]{:T(128)} %convert_element_type.114, (f32[2,512]{1,0:T(2,128)S(1)}, f32[2,512]{1,0:T(2,128)S(1)}, f32[2,512,128]{2,1,0:T(8,128)S(1)}) %tuple.53, (s32[]{:T(128)}, s32[]{:T(128)}, s32[]{:T(128)}, ...), branch_computations={%region_4.4_spmd, %region_5.0_spmd} | conditional | flops 274729984 | bytes 9005188 | solution.py:79
  216.1 0.2 broadcast_compare_fusion
  216.4 1.6 fusion.41
  218.0 0.4 fusion.5
  218.4 1.7 convolution_add_fusion
  224.3 0.2 divide_convert_fusion
  224.5 1.0 copy.58
  225.5 3.6 all-to-all-start
  229.1 58.9 %reduce-scatter.2.cloned.1.call-done = bf16[128,4,2048]{2,0,1:T(8,128)(2,1)} async-done(((bf16[512,4,2048]{2,0,1:T(8,128)(2,1)}), bf16[128,4,2048]{2,0,1:T(8,128)(2,1)}) %reduce-scatter.2.cloned.1.call-update) | async-done | bytes 2097168 | tf_op jit(solution)/shard_map/reduce_scatter | solution.py:135
  288.0 4.6 %copy.66 = bf16[128,4,2048]{2,1,0:T(4,128)(2,1)} copy(bf16[128,4,2048]{2,0,1:T(8,128)(2,1)} %reduce-scatter.2.cloned.1.call-done) | data formatting | bytes 4194304 | tf_op jit(solution)/shard_map/reduce_scatter | solution.py:135
  292.6 0.0 all-to-all-done
  292.6 8.5 %all-to-all-start.2 = ((bf16[128,4,2048]{2,1,0:T(4,128)(2,1)}), bf16[128,4,2048]{2,1,0:T(4,128)(2,1)S(1)}, u32[]{:S(2)}, u32[]{:S(2)}) async-start(bf16[128,4,2048]{2,1,0:T(4,128)(2,1)} %copy.66), calls=%async_computation.3 | async-start | bytes 4194304 | tf_op jit(solution)/shard_map/all_to_all | solution.py:143
  301.1 0.1 copy.68
  301.2 3.7 %fusion.17 = bf16[128,2048]{1,0:T(8,128)(2,1)} fusion(bf16[8,128,128]{2,1,0:T(8,128)(2,1)S(1)} %bitcast.110, bf16[8,128,2048]{2,1,0:T(8,128)(2,1)} %bitcast.109), kind=kOutput, calls=%fused_computation.30 | convolution fusion | flops 537133056 | bytes 4980736 | tf_op jit(solution)/shard_map/hqd,hde->qe/dot_general | solution.py:128
  304.9 44.2 %all-to-all-done.2 = bf16[128,4,2048]{2,1,0:T(4,128)(2,1)S(1)} async-done(((bf16[128,4,2048]{2,1,0:T(4,128)(2,1)}), bf16[128,4,2048]{2,1,0:T(4,128)(2,1)S(1)}, u32[]{:S(2)}, u32[]{:S(2)}) %all-to-all-start.2) | async-done | bytes 2097184 | tf_op jit(solution)/shard_map/all_to_all | solution.py:143
  349.1 2.4 copy.73
  351.5 2.5 reshape.156
  354.0 1.4 gather_fusion.2
  355.4 1.3 reshape.158
  356.7 4.0 %multiply_reduce_fusion = bf16[128,2048]{1,0:T(8,128)(2,1)} fusion(f32[128,2,2048]{2,1,0:T(2,128)S(1)} %reshape.158, f32[128,2]{1,0:T(8,128)S(1)} %copy.68), kind=kLoop, calls=%fused_computation.39 | loop fusion | flops 786432 | bytes 2622464 | tf_op jit(solution)/shard_map/reduce_sum | solution.py:150
  (47 shorter events, 0.4 us)
Async XLA Ops:
  7.2 124.1 %all-gather.8.cloned.1.call-start = ((), (), s32[]{:S(2)}) async-start(), calls=%async_computation.6 | async-start | bytes 10485760 | tf_op jit(solution)/shard_map/all_gather | solution.py:131
  73.8 0.9 copy-start
  73.8 1.1 copy-start.4
  73.8 100.4 %all-gather.4.cloned.1.call-start = ((), (), s32[]{:S(2)}) async-start(), calls=%async_computation.4 | async-start | bytes 1179648 | tf_op jit(solution)/shard_map/all_gather | solution.py:40
  75.7 139.7 %all-gather.6.cloned.1.call-start = ((), (), s32[]{:S(2)}) async-start(), calls=%async_computation.5 | async-start | bytes 1179648 | tf_op jit(solution)/shard_map/all_gather | solution.py:41
  76.5 211.6 %reduce-scatter.2.cloned.1.call-start = ((), (), s32[]{:S(2)}) async-start(), calls=%async_computation.7 | async-start | bytes 10485760 | tf_op jit(solution)/shard_map/reduce_scatter | solution.py:135
  152.2 0.8 copy-start.2
  152.2 3.3 copy-start.1
  152.2 3.6 copy-start.5
  225.5 67.1 %all-to-all-start = ((bf16[2,512,128]{2,0,1:T(2,128)(2,1)}), bf16[2,512,128]{2,0,1:T(2,128)(2,1)S(1)}, u32[]{:S(2)}, u32[]{:S(2)}) async-start(bf16[2,512,128]{2,0,1:T(2,128)(2,1)} %copy.58), calls=%async_computation | async-start | bytes 524288 | tf_op jit(solution)/shard_map/all_to_all | solution.py:125
  292.6 8.5 %copy-start.3 = (f32[128,2]{0,1:T(2,128)S(1)}, f32[128,2]{0,1:T(2,128)}, u32[]{:S(2)}) copy-start(f32[128,2]{0,1:T(2,128)} %param.28) | copy-start | bytes 3076
  292.6 56.5 %all-to-all-start.2 = ((bf16[128,4,2048]{2,1,0:T(4,128)(2,1)}), bf16[128,4,2048]{2,1,0:T(4,128)(2,1)S(1)}, u32[]{:S(2)}, u32[]{:S(2)}) async-start(bf16[128,4,2048]{2,1,0:T(4,128)(2,1)} %copy.66), calls=%async_computation.3 | async-start | bytes 4194304 | tf_op jit(solution)/shard_map/all_to_all | solution.py:143
Sparse Core Ops, SparseCore 0:
  74.0 57.2 all-gather.7
  134.0 40.2 all-gather.3
  176.4 38.9 all-gather.5
  217.9 70.0 reduce-scatter.1
where the time goes:
time: 368 us; the launch traced here: 367 us
  waiting for transfers between devices  218 us (59%)
  blocking collectives  55.3 us (15%)
  matrix products  27.9 us (8%)
  local copies, waits for them, and re-layouts  25 us (7%)
  between operations  14 us (4%)
  starting transfers between devices  12.5 us (3%)
  other arithmetic  10.1 us (3%)
  loops' own time  4.82 us (1%)
    reduce_scatter x1, waiting for transfers between devices, on_device(): lax.psum_scatter(jnp.einsum('ref,edf->red', hidden, w_down, preferred_ele...  58.9 us
    all_to_all x1, blocking collectives, dispatch(): lax.all_to_all(outgoing, 'ep', split_axis=1, concat_axis=0, tiled=True)  55.3 us
    all_gather x1, waiting for transfers between devices, on_device(): pieces = lax.all_gather(received, 'tp', axis=0, tiled=True)  54.6 us
    all_to_all x1, waiting for transfers between devices, on_device(): lax.all_to_all(summed, 'ep', split_axis=0, concat_axis=1, tiled=True)  44.2 us
    all_gather x1, waiting for transfers between devices, attend(): value_rows = lax.all_gather(values, 'ep', axis=0, tiled=True)  41.2 us
    all_gather x1, waiting for transfers between devices, attend(): key_matrix_rows = lax.all_gather(normed_k, 'ep', axis=0, tiled=True)  18.2 us
    dot_general x1, matrix products, on_device(): jnp.einsum('ref,edf->red', hidden, w_down, preferred_element_type=jnp.flo...  14 us
    all_to_all x1, starting transfers between devices, on_device(): lax.all_to_all(summed, 'ep', split_axis=0, concat_axis=1, tiled=True)  8.48 us
  transfers between devices with their start and end apart: 6, of which 5 were waited for; matrix products, arithmetic and copies ran while one was open for 10% of the time, Pallas kernels for 0%

commit v1 on v0

--- a/solution.py
+++ b/solution.py
@@ -140,7 +140,12 @@
         scatter_dimension=0,
         tiled=True,
     )
-    returned = lax.all_to_all(summed, "ep", split_axis=0, concat_axis=1, tiled=True)
+    returned = jnp.concatenate(
+        jax.lax.all_to_all(
+            jnp.stack(jnp.split(summed, jax.lax.axis_size("ep"), 0), axis=0), "ep", 0, 0
+        ),
+        1,
+    )
     flat_back = returned.reshape(-1, returned.shape[2])
     picked = (
         flat_back[slots]

time: 368 us -> 373 us (1.014)
  local copies, waits for them, and re-layouts: 25 us -> 30.1 us
    unnamed x18 -> x27, local copies, waits for them, and re-layouts: 3.55 us -> 11.7 us
    reduce_scatter x1 -> x0, local copies, waits for them, and re-layouts: 4.56 us -> none  [on_device(): lax.psum_scatter(jnp.einsum('ref,edf->red', hidden, w_down, preferred_ele...]
  transfers between devices with their start and end apart: 6 -> 6, of which waited for: 5 -> 5; matrix products, arithmetic and copies ran while one was open for 10% -> 11% of each run, Pallas kernels for 0% -> 0%
where the time goes in v1:
time: 373 us; the launch traced here: 372 us
  waiting for transfers between devices  218 us (58%)
  blocking collectives  55.3 us (15%)
  local copies, waits for them, and re-layouts  30.1 us (8%)
  matrix products  27.8 us (7%)
  between operations  14.1 us (4%)
  starting transfers between devices  12.2 us (3%)
  other arithmetic  9.95 us (3%)
  loops' own time  4.82 us (1%)
    reduce_scatter x1, waiting for transfers between devices, on_device(): lax.psum_scatter(jnp.einsum('ref,edf->red', hidden, w_down, preferred_ele...  59.1 us
    all_to_all x1, blocking collectives, dispatch(): lax.all_to_all(outgoing, 'ep', split_axis=1, concat_axis=0, tiled=True)  55.3 us
    all_gather x1, waiting for transfers between devices, on_device(): pieces = lax.all_gather(received, 'tp', axis=0, tiled=True)  54.6 us
    all_to_all x1, waiting for transfers between devices, on_device(): jax.lax.all_to_all(jnp.stack(jnp.split(summed, jax.lax.axis_size('ep'), 0...  44.2 us
    all_gather x1, waiting for transfers between devices, attend(): value_rows = lax.all_gather(values, 'ep', axis=0, tiled=True)  41.2 us
    all_gather x1, waiting for transfers between devices, attend(): key_matrix_rows = lax.all_gather(normed_k, 'ep', axis=0, tiled=True)  18.3 us
    dot_general x1, matrix products, on_device(): jnp.einsum('ref,edf->red', hidden, w_down, preferred_element_type=jnp.flo...  13.9 us
    unnamed x27, local copies, waits for them, and re-layouts  11.7 us
  transfers between devices with their start and end apart: 6, of which 5 were waited for; matrix products, arithmetic and copies ran while one was open for 11% of the time, Pallas kernels for 0%

profile of v1, /device:TPU:0, one launch (start us, length us, event | category | flops | bytes accessed | tf_op | source)
XLA Modules:
  0.0 372.4 jit_solution(14994282255550130991)
XLA Ops:
  7.2 0.8 copy.58
  8.0 0.1 eq.29
  8.1 0.1 eq.25
  8.3 0.1 reshape.153
  8.4 0.6 reduce-window.6
  9.0 0.2 slice_reduce_fusion
  9.3 0.1 fusion.41
  9.4 1.4 scatter_custom_fusion
  10.8 1.2 fusion.22
  12.1 1.2 fusion.24
  13.4 2.5 gather_fusion.1
  15.8 1.2 copy.62
  17.0 55.3 %all_to_all.41 = bf16[16,32,2048]{2,0,1:T(8,128)(2,1)S(1)} all-to-all(bf16[16,32,2048]{2,0,1:T(8,128)(2,1)S(1)} %copy.62), channel_id=1, replica_groups=mesh['ep'=8,'tp'=4] {'ep'}, dimensions={1} | all-to-all | bytes 4194304 | tf_op jit(solution)/shard_map/all_to_all | solution.py:103
  72.3 1.5 copy.63
  73.8 0.0 all-gather.4.cloned.1.call-start
  73.9 0.8 copy-done.1
  74.7 0.1 fusion.28
  74.9 0.8 fusion.30
  75.7 0.0 all-gather.6.cloned.1.call-start
  75.8 0.7 all-gather.6.cloned.1.call-update
  76.4 0.2 reduce-scatter.2.cloned.1.call-start
  76.7 54.6 %all-gather.8.cloned.1.call-done = bf16[512,4,2048]{2,0,1:T(8,128)(2,1)} async-done(((bf16[128,4,2048]{2,0,1:T(8,128)(2,1)}), bf16[512,4,2048]{2,0,1:T(8,128)(2,1)}) %all-gather.8.cloned.1.call-update) | async-done | bytes 8388624 | tf_op jit(solution)/shard_map/all_gather | solution.py:131
  131.3 6.9 %fusion.50 = f32[4,512,256]{2,1,0:T(8,128)S(1)} fusion(bf16[512,4,2048]{2,0,1:T(8,128)(2,1)} %all-gather.8.cloned.1.call-done, bf16[4,2048,256]{2,1,0:T(8,128)(2,1)} %param.29), kind=kOutput, calls=%fused_computation.104 | convolution fusion | flops 2147483648 | bytes 14680064 | tf_op jit(solution)/shard_map/red,edf->ref/dot_general | solution.py:132
  138.2 13.9 %convert_bitcast_fusion = bf16[512,4,2048]{2,0,1:T(8,128)(2,1)} fusion(bf16[4,2048,256]{2,1,0:T(8,128)(2,1)} %param.31, f32[4,512,256]{2,1,0:T(8,128)S(1)} %fusion.50, bf16[512,4,2048]{2,0,1:T(8,128)(2,1)} %all-gather.8.cloned.1.call-done, bf16[4,2048,256]{2,1,0:T(8,128)(2,1)} %param.30), kind=kOutput, calls=%fused_computation.28 | convolution fusion | flops 4302307328 | bytes 27262976 | tf_op jit(solution)/shard_map/ref,edf->red/dot_general | solution.py:136
  152.1 0.7 copy-done.3
  152.8 0.7 copy.53
  153.5 0.6 fusion.43
  154.1 1.0 gather_fusion
  155.2 0.1 select_bitcast_fusion
  155.3 0.1 copy.55
  155.4 0.1 copy.52
  155.6 0.1 fusion.25
  155.7 0.1 fusion.27
  155.8 0.2 copy.54
  156.0 18.3 %all-gather.4.cloned.1.call-done = bf16[4096,128]{1,0:T(8,128)(2,1)} async-done(((bf16[512,128]{1,0:T(8,128)(2,1)}), bf16[4096,128]{1,0:T(8,128)(2,1)}) %all-gather.4.cloned.1.call-update) | async-done | bytes 1048592 | tf_op jit(solution)/shard_map/all_gather | solution.py:40
  174.3 41.2 %all-gather.6.cloned.1.call-done = bf16[4096,128]{1,0:T(8,128)(2,1)} async-done(((bf16[512,128]{1,0:T(8,128)(2,1)}), bf16[4096,128]{1,0:T(8,128)(2,1)}) %all-gather.6.cloned.1.call-update) | async-done | bytes 1048592 | tf_op jit(solution)/shard_map/all_gather | solution.py:41
  215.5 8.8 %while.18 = (s32[]{:T(128)}, f32[2,512]{1,0:T(2,128)S(1)}, f32[2,512]{1,0:T(2,128)S(1)}, f32[2,512,128]{2,1,0:T(8,128)S(1)}, s32[]{:T(128)}, /*index=5*/bf16[409...) while((s32[]{:T(128)}, f32[2,512]{1,0:T(2,128)S(1)}, ...), condition=%wide.region_8.9_spmd.clone, body=%wide.region_3.8_spmd.clone.sunk | while | flops 274729984 | bytes 9007507 | solution.py:81
  216.1 4.1 %conditional.3 = ((f32[2,512]{1,0:T(2,128)S(1)}, f32[2,512]{1,0:T(2,128)S(1)}, f32[2,512,128]{2,1,0:T(8,128)S(1)})) conditional(s32[]{:T(128)} %convert_element_type.114, (f32[2,512]{1,0:T(2,128)S(1)}, f32[2,512]{1,0:T(2,128)S(1)}, f32[2,512,128]{2,1,0:T(8,128)S(1)}) %tuple.54, (s32[]{:T(128)}, s32[]{:T(128)}, s32[]{:T(128)}, ...), branch_computations={%region_4.4_spmd, %region_5.0_spmd} | conditional | flops 274729984 | bytes 9005188 | solution.py:79
  216.1 0.2 broadcast_compare_fusion
  216.4 1.6 fusion.49
  218.0 0.4 fusion.5
  218.4 1.7 convolution_add_fusion
  224.3 0.2 divide_convert_fusion
  224.5 1.0 copy.56
  225.5 3.4 all-to-all-start
  229.0 59.1 %reduce-scatter.2.cloned.1.call-done = bf16[128,4,2048]{2,0,1:T(8,128)(2,1)} async-done(((bf16[512,4,2048]{2,0,1:T(8,128)(2,1)}), bf16[128,4,2048]{2,0,1:T(8,128)(2,1)}) %reduce-scatter.2.cloned.1.call-update) | async-done | bytes 2097168 | tf_op jit(solution)/shard_map/reduce_scatter | solution.py:135
  288.0 1.0 fusion.38
  289.0 1.0 fusion.37
  290.0 1.0 fusion.36
  290.9 1.0 fusion.35
  291.9 1.0 fusion.34
  292.9 1.0 fusion.33
  293.9 1.0 fusion.32
  294.8 1.0 fusion.31
  295.8 1.3 copy-done
  297.2 8.5 %all-to-all-start.2 = ((bf16[8,16,4,2048]{3,1,2,0:T(8,128)(2,1)}), bf16[8,16,4,2048]{3,1,2,0:T(8,128)(2,1)S(1)}, u32[]{:S(2)}, u32[]{:S(2)}) async-start(bf16[8,16,4,2048]{3,1,2,0:T(8,128)(2,1)} %copy-done), calls=%async_computation.3 | async-start | bytes 4194304 | tf_op jit(solution)/shard_map/all_to_all | solution.py:144
  305.7 0.1 copy.65
  305.8 3.7 %fusion.17 = bf16[128,2048]{1,0:T(8,128)(2,1)} fusion(bf16[8,128,128]{2,1,0:T(8,128)(2,1)S(1)} %bitcast.138, bf16[8,128,2048]{2,1,0:T(8,128)(2,1)} %bitcast.137), kind=kOutput, calls=%fused_computation.30 | convolution fusion | flops 537133056 | bytes 4980736 | tf_op jit(solution)/shard_map/hqd,hde->qe/dot_general | solution.py:128
  309.6 44.2 %all-to-all-done.2 = bf16[8,16,4,2048]{3,1,2,0:T(8,128)(2,1)S(1)} async-done(((bf16[8,16,4,2048]{3,1,2,0:T(8,128)(2,1)}), bf16[8,16,4,2048]{3,1,2,0:T(8,128)(2,1)S(1)}, u32[]{:S(2)}, u32[]{:S(2)}) %all-to-all-start.2) | async-done | bytes 2097184 | tf_op jit(solution)/shard_map/all_to_all | solution.py:144
  353.7 3.0 copy.64
  356.7 2.5 reshape_reshape.3
  359.2 1.4 gather_fusion.2
  360.6 1.3 reshape.157
  361.9 3.9 %multiply_reduce_fusion = bf16[128,2048]{1,0:T(8,128)(2,1)} fusion(f32[128,2,2048]{2,1,0:T(2,128)S(1)} %reshape.157, f32[128,2]{1,0:T(8,128)S(1)} %copy.65), kind=kLoop, calls=%fused_computation.38 | loop fusion | flops 786432 | bytes 2622464 | tf_op jit(solution)/shard_map/reduce_sum | solution.py:155
  (55 shorter events, 0.5 us)
Async XLA Ops:
  7.2 124.1 %all-gather.8.cloned.1.call-start = ((), (), s32[]{:S(2)}) async-start(), calls=%async_computation.6 | async-start | bytes 10485760 | tf_op jit(solution)/shard_map/all_gather | solution.py:131
  73.8 0.9 copy-start.1
  73.8 1.1 copy-start.5
  73.8 100.4 %all-gather.4.cloned.1.call-start = ((), (), s32[]{:S(2)}) async-start(), calls=%async_computation.4 | async-start | bytes 1179648 | tf_op jit(solution)/shard_map/all_gather | solution.py:40
  75.7 139.7 %all-gather.6.cloned.1.call-start = ((), (), s32[]{:S(2)}) async-start(), calls=%async_computation.5 | async-start | bytes 1179648 | tf_op jit(solution)/shard_map/all_gather | solution.py:41
  76.4 211.6 %reduce-scatter.2.cloned.1.call-start = ((), (), s32[]{:S(2)}) async-start(), calls=%async_computation.7 | async-start | bytes 10485760 | tf_op jit(solution)/shard_map/reduce_scatter | solution.py:135
  152.1 0.8 copy-start.3
  152.1 3.3 copy-start.2
  152.1 3.6 copy-start.6
  225.5 71.7 %all-to-all-start = ((bf16[2,512,128]{2,0,1:T(2,128)(2,1)}), bf16[2,512,128]{2,0,1:T(2,128)(2,1)S(1)}, u32[]{:S(2)}, u32[]{:S(2)}) async-start(bf16[2,512,128]{2,0,1:T(2,128)(2,1)} %copy.56), calls=%async_computation | async-start | bytes 524288 | tf_op jit(solution)/shard_map/all_to_all | solution.py:125
  295.8 1.4 copy-start
  297.2 8.5 %copy-start.4 = (f32[128,2]{0,1:T(2,128)S(1)}, f32[128,2]{0,1:T(2,128)}, u32[]{:S(2)}) copy-start(f32[128,2]{0,1:T(2,128)} %param.28) | copy-start | bytes 3076
  297.2 56.5 %all-to-all-start.2 = ((bf16[8,16,4,2048]{3,1,2,0:T(8,128)(2,1)}), bf16[8,16,4,2048]{3,1,2,0:T(8,128)(2,1)S(1)}, u32[]{:S(2)}, u32[]{:S(2)}) async-start(bf16[8,16,4,2048]{3,1,2,0:T(8,128)(2,1)} %copy-done), calls=%async_computation.3 | async-start | bytes 4194304 | tf_op jit(solution)/shard_map/all_to_all | solution.py:144
Sparse Core Ops, SparseCore 0:
  74.0 57.2 all-gather.7
  134.0 40.2 all-gather.3
  176.4 38.9 all-gather.5
  217.9 70.0 reduce-scatter.1
